TPU v7x, 32 devices: a whole 2x2x4 slice. The times are simulated.
32 devices in a mesh: dp: 4 (over y, x), kv: 4 (over z), tp: 2 (over core).
Axes of the slice: x: 2, y: 2, z: 4, core: 2. Of those that a mesh axis runs over, the one named last changes fastest.
Arguments:
- piece_tokens: bfloat16 [2048, 2048], P(('dp', 'kv')), parts along dimension 0, may hold values from -6 to 6
- step_tokens: bfloat16 [16, 2048], P(('dp', 'kv')), parts along dimension 0, may hold values from -6 to 6
- norm_gain: float32 [2048], replicated, may hold values from 0.1 to 1.9
- query_weight: bfloat16 [2048, 1024], P(None, 'tp'), may hold values from -0.125 to 0.125
- key_weight: bfloat16 [2048, 1024], P(None, 'tp'), may hold values from -0.125 to 0.125
- value_weight: bfloat16 [2048, 1024], P(None, 'tp'), may hold values from -0.125 to 0.125
- gate_weight: bfloat16 [2048, 16], replicated, may hold values from -0.125 to 0.125
- gate_bias: float32 [16], replicated, may hold values from 3 to 10.5
- out_weight: bfloat16 [1024, 2048], P(None, 'tp'), may hold values from -0.1875 to 0.1875
- cache_keys: bfloat16 [8192, 1024], P(('dp', 'kv'), 'tp'), parts along dimension 0, may hold values from -320 to 320
- cache_values: bfloat16 [8192, 1024], P(('dp', 'kv'), 'tp'), parts along dimension 0, may hold values from -10 to 10
- cache_decay: float32 [16, 8192], P('tp', ('dp', 'kv')), parts along dimension 1, may hold values from -696.32 to 0, as said below
- decay_total: float32 [64], P('dp'), parts along dimension 0, may hold values from -696.32 to 0, as said below
- step_keys: bfloat16 [16, 1024, 1024], P(('dp', 'kv'), None, 'tp'), parts along dimension 0, may hold values from -6 to 6
- step_values: bfloat16 [16, 1024, 1024], P(('dp', 'kv'), None, 'tp'), parts along dimension 0, may hold values from -6 to 6
- step_gates: float32 [16, 16, 1024], P(('dp', 'kv'), 'tp'), parts along dimension 0, may hold values from -0.34 to 0
- step_lengths: int32 [16], P(('dp', 'kv')), parts along dimension 0, may hold values from 1 to 1024, 2048 in all
Outputs:
- piece_out: bfloat16 [2048, 2048], P(('dp', 'kv'), 'tp'), parts along dimension 0
- step_out: bfloat16 [16, 2048], P(('dp', 'kv'), 'tp'), parts along dimension 0
There are 4 independent parts, one for each index of `dp`. A program takes and returns all parts, laid end to end along the dimension named above; an argument that names none is the same for every part. Nothing has to cross between parts.
Inputs may be any that keep to these rules, and one draw needn't show every extreme that they name: `cache_decay`: cumulative values never rise along the positions and start at one gate below zero. `decay_total`: equal to the cumulative value of the last cached position. `step_lengths`: each length is 1 to 1024; the largest is exactly 1024; positions at or past a length are unused.
All inputs are finite; a program needn't handle non-finite values.
Results may differ from a plain program's by a relative error of at most 0.0095.
The roundings to bfloat16 on the way count: a program that leaves them out, or rounds other values in their place, can miss the bound.
Values may be sent and summed in bfloat16 or wider, within the bound.
A program may use at most 128 MiB of HBM per device.

v0:
```python
import jax
import jax.numpy as jnp
from jax import lax
from jax.sharding import PartitionSpec as P

norm_eps = 1e-06
negative = -1e30


def carried_in(value, axis, join, neutral):
    count, mine = (lax.axis_size(axis), lax.axis_index(axis))
    pieces = lax.all_gather(value, axis)
    total = jnp.full_like(value, 0) + jnp.asarray(neutral, value.dtype)

    def step(position, total):
        longer = join(total, pieces[position])
        return jnp.where(position < mine, longer, total)

    return lax.fori_loop(0, count - 1, step, total)


def normalize(token_rows, norm_gain):
    wide = token_rows.astype(jnp.float32)
    factor = lax.rsqrt(jnp.mean(wide * wide, axis=-1, keepdims=True) + norm_eps)
    return (wide * factor * norm_gain).astype(jnp.bfloat16)


def attend_piece(queries, positions, all_keys, all_values, key_bias, key_slots, cache_len):
    head_count = key_bias.shape[0]
    query_count = queries.shape[0]
    head_width = all_keys.shape[1] // head_count
    score_scale = head_width ** (-0.5)
    key_heads = all_keys.reshape(all_keys.shape[0], head_count, head_width)
    value_heads = all_values.reshape(all_values.shape[0], head_count, head_width)

    def one_block(block_args):
        block_q, block_pos = block_args
        row_count = block_q.shape[0]
        scores = (
            jnp.einsum(
                "qhd,khd->hqk",
                block_q.reshape(row_count, head_count, head_width),
                key_heads,
                preferred_element_type=jnp.float32,
            )
            * score_scale
        )
        scores = scores + key_bias[:, None, :]
        visible = jnp.concatenate(
            [jnp.ones((row_count, cache_len), jnp.bool_), block_pos[:, None] >= key_slots[None, :]],
            axis=1,
        )
        scores = jnp.where(visible[None], scores, negative)
        row_high = jnp.max(scores, axis=-1)
        exp_scores = jnp.exp(scores - row_high[..., None])
        row_mass = jnp.sum(exp_scores, axis=-1)
        summed = jnp.einsum(
            "hqk,khd->qhd",
            exp_scores.astype(jnp.bfloat16),
            value_heads,
            preferred_element_type=jnp.float32,
        )
        part_means = (
            (summed / row_mass.T[:, :, None])
            .astype(jnp.bfloat16)
            .reshape(row_count, head_count * head_width)
        )
        return (part_means, row_high.T, row_mass.T)

    if query_count > 512 and query_count % 512 == 0:
        group_count = query_count // 512
        part_means, part_high, part_mass = lax.map(
            one_block, (queries.reshape(group_count, 512, -1), positions.reshape(group_count, 512))
        )
        return (
            part_means.reshape(query_count, -1),
            part_high.reshape(query_count, head_count),
            part_mass.reshape(query_count, head_count),
        )
    return one_block((queries, positions))


def combine(part_means, part_high, part_mass):
    best_high = jnp.max(part_high, axis=0)
    share = part_mass * jnp.exp(part_high - best_high[None])
    peer_count, row_count, head_count = share.shape
    part_float = part_means.reshape(peer_count, row_count, head_count, -1).astype(jnp.float32)
    summed = jnp.sum(share[..., None] * part_float, axis=0) / jnp.sum(share, axis=0)[..., None]
    return summed.astype(jnp.bfloat16).reshape(row_count, -1)


def per_device(
    piece_tokens,
    step_tokens,
    norm_gain,
    query_weight,
    key_weight,
    value_weight,
    gate_weight,
    gate_bias,
    out_weight,
    cache_keys,
    cache_values,
    cache_decay,
    decay_total,
    step_keys,
    step_values,
    step_gates,
    step_lengths,
):
    piece_rows = piece_tokens.shape[0]
    step_count = step_tokens.shape[0]
    head_count = cache_decay.shape[0]
    head_width = query_weight.shape[1] // head_count
    score_scale = head_width ** (-0.5)
    head_start = lax.axis_index("tp") * head_count
    token_rows = jnp.concatenate([piece_tokens, step_tokens], axis=0)
    normed = normalize(token_rows, norm_gain)
    queries = jnp.dot(normed, query_weight, preferred_element_type=jnp.float32).astype(jnp.bfloat16)
    new_keys = jnp.dot(normed, key_weight, preferred_element_type=jnp.float32).astype(jnp.bfloat16)
    new_values = jnp.dot(normed, value_weight, preferred_element_type=jnp.float32).astype(
        jnp.bfloat16
    )
    gate_cols = lax.dynamic_slice_in_dim(gate_weight, head_start, head_count, 1)
    bias_cols = lax.dynamic_slice_in_dim(gate_bias, head_start, head_count, 0)
    start_decay = lax.dynamic_slice_in_dim(decay_total, head_start, head_count, 0)
    log_gates = jax.nn.log_sigmoid(
        jnp.dot(normed, gate_cols, preferred_element_type=jnp.float32) + bias_cols
    )
    piece_gates = log_gates[:piece_rows]
    gate_before = carried_in(
        jnp.sum(piece_gates, axis=0), "kv", jnp.add, jnp.zeros((head_count,), jnp.float32)
    )
    piece_decay = start_decay + gate_before + jnp.cumsum(piece_gates, axis=0)
    key_bias = -jnp.concatenate([cache_decay, piece_decay.T], axis=1)
    all_keys = jnp.concatenate([cache_keys, new_keys[:piece_rows]], axis=0)
    all_values = jnp.concatenate([cache_values, new_values[:piece_rows]], axis=0)
    key_slots = lax.axis_index("kv") * piece_rows + jnp.arange(piece_rows, dtype=jnp.int32)
    cache_len = cache_keys.shape[0]
    peer_count = lax.axis_size("kv")
    own_queries = queries[:piece_rows]
    gathered = lax.all_gather(own_queries, "kv", axis=0, tiled=True)
    positions = jnp.arange(peer_count * piece_rows, dtype=jnp.int32)
    part_means, part_high, part_mass = attend_piece(
        gathered, positions, all_keys, all_values, key_bias, key_slots, cache_len
    )
    part_means = lax.all_to_all(part_means[None], "kv", split_axis=1, concat_axis=0, tiled=True)
    part_high, part_mass = (
        lax.all_to_all(part_high[None], "kv", split_axis=1, concat_axis=0, tiled=True),
        lax.all_to_all(part_mass[None], "kv", split_axis=1, concat_axis=0, tiled=True),
    )
    piece_att = combine(part_means, part_high, part_mass)
    cache_span = step_keys.shape[1]
    step_q = queries[piece_rows:].reshape(step_count, head_count, head_width)
    step_k = new_keys[piece_rows:].reshape(step_count, head_count, head_width)
    step_v = new_values[piece_rows:].reshape(step_count, head_count, head_width)
    step_lg = log_gates[piece_rows:]
    in_cache = jnp.arange(cache_span, dtype=jnp.int32)[None, :] < step_lengths[:, None]
    kept_gates = jnp.where(in_cache[:, None, :], step_gates, 0.0)
    running = jnp.cumsum(kept_gates, axis=2)
    after_sum = running[:, :, -1:] - running
    cache_scores = (
        jnp.einsum(
            "bhd,blhd->bhl",
            step_q,
            step_keys.reshape(step_count, cache_span, head_count, head_width),
            preferred_element_type=jnp.float32,
        )
        * score_scale
    )
    cache_scores = cache_scores + step_lg[:, :, None] + after_sum
    cache_scores = jnp.where(in_cache[:, None, :], cache_scores, negative)
    self_scores = (
        jnp.einsum("bhd,bhd->bh", step_q, step_k, preferred_element_type=jnp.float32) * score_scale
    )
    step_high = jnp.maximum(jnp.max(cache_scores, axis=-1), self_scores)
    cache_exp = jnp.exp(cache_scores - step_high[..., None])
    self_exp = jnp.exp(self_scores - step_high)
    step_mass = jnp.sum(cache_exp, axis=-1) + self_exp
    step_mix = jnp.einsum(
        "bhl,blhd->bhd",
        cache_exp.astype(jnp.bfloat16),
        step_values.reshape(step_count, cache_span, head_count, head_width),
        preferred_element_type=jnp.float32,
    )
    step_mix = step_mix + self_exp.astype(jnp.bfloat16).astype(jnp.float32)[
        ..., None
    ] * step_v.astype(jnp.float32)
    step_att = (
        (step_mix / step_mass[..., None])
        .astype(jnp.bfloat16)
        .reshape(step_count, head_count * head_width)
    )
    att_rows = jnp.concatenate([piece_att, step_att], axis=0)
    projected = jnp.dot(
        lax.all_gather(att_rows, "tp", axis=1, tiled=True),
        out_weight,
        preferred_element_type=jnp.float32,
    )
    projected = projected.astype(jnp.bfloat16)
    return (projected[:piece_rows], projected[piece_rows:])


def solution(mesh):
    in_specs = (
        P(("dp", "kv"), None),
        P(("dp", "kv"), None),
        P(),
        P(None, "tp"),
        P(None, "tp"),
        P(None, "tp"),
        P(),
        P(),
        P(None, "tp"),
        P(("dp", "kv"), "tp"),
        P(("dp", "kv"), "tp"),
        P("tp", ("dp", "kv")),
        P("dp"),
        P(("dp", "kv"), None, "tp"),
        P(("dp", "kv"), None, "tp"),
        P(("dp", "kv"), "tp", None),
        P(("dp", "kv")),
    )
    out_specs = (P(("dp", "kv"), "tp"), P(("dp", "kv"), "tp"))
    return jax.shard_map(
        per_device, mesh=mesh, in_specs=in_specs, out_specs=out_specs, check_vma=False
    )
```

profile of v0, /device:TPU:0, one launch (start us, length us, event | category | flops | bytes accessed | tf_op | source)
XLA Modules:
  0.0 125.6 jit_solution(8513010429715983522)
XLA Ops:
  0.7 1.4 %fusion.9 = f32[129]{0:T(256)S(1)} fusion(bf16[1,2048]{1,0:T(2,128)(2,1)} %param.20, bf16[128,2048]{1,0:T(8,128)(2,1)} %param.19), kind=kLoop, calls=%fused_computation.16 | loop fusion | flops 1585023 | bytes 528900 | tf_op jit(solution)/shard_map/reduce_sum | solution.py:24
  2.9 1.5 %fusion.25 = f32[129,8]{0,1:T(8,128)S(1)} fusion(bf16[2048,16]{0,1:T(8,128)(2,1)} %param.25, s32[]{:T(128)S(6)} %select_n.43, f32[8]{0:T(128)S(1)} %dynamic_slice.18, f32[2048]{0:T(1024)} %param.21, f32[129]{0:T(256)S(1)} %add_rsqrt_fusion, bf16[1,2048]{1,0:T(2,128)(2,1)} %param.20, bf16[128,2048]{1,0:T(8,128)(2,1)} %param.19), kind=kOutput, calls=%fused_computation.49 | convolution fusion | flops 6085704 | bytes 578120 | tf_op jit(solution)/shard_map/dot_general | solution.py:128
  6.1 13.5 %all-reduce.1 = f32[32]{0:T(128)S(1)} all-reduce(f32[32]{0:T(128)S(1)} %dynamic-update-slice), channel_id=2, replica_groups=mesh['dp'=4,'kv'=4,'tp'=2] {'kv'}, use_global_device_ids=true, to_apply=%add.1 | all-reduce | flops 32 | bytes 256
  20.3 2.1 %convolution_convert_fusion.2 = bf16[129,512]{1,0:T(8,128)(2,1)S(1)} fusion(bf16[2048,512]{1,0:T(8,128)(2,1)} %param.23, f32[2048]{0:T(1024)S(1)} %copy-done.20, f32[129]{0:T(256)S(1)} %add_rsqrt_fusion, bf16[1,2048]{1,0:T(2,128)(2,1)S(1)} %copy-done.13, bf16[128,2048]{1,0:T(8,128)(2,1)S(1)} %copy-done.3), kind=kOutput, calls=%fused_computation.14 | convolution fusion | flops 272448000 | bytes 2766340 | tf_op jit(solution)/shard_map/dot_general | solution.py:120
  23.5 2.3 %convolution_convert_fusion.3 = bf16[129,512]{1,0:T(8,128)(2,1)S(1)} fusion(bf16[2048,512]{1,0:T(8,128)(2,1)} %param.22, f32[2048]{0:T(1024)S(1)} %copy-done.20, f32[129]{0:T(256)S(1)} %add_rsqrt_fusion, bf16[1,2048]{1,0:T(2,128)(2,1)S(1)} %copy-done.13, bf16[128,2048]{1,0:T(8,128)(2,1)} %param.19), kind=kOutput, calls=%fused_computation.15 | convolution fusion | flops 272448000 | bytes 2766340 | tf_op jit(solution)/shard_map/dot_general | solution.py:119
  26.5 14.8 %all_gather.12 = bf16[512,512]{1,0:T(8,128)(2,1)S(1)} all-gather(bf16[128,512]{1,0:T(8,128)(2,1)S(1)} %slice.52), channel_id=1, replica_groups=mesh['dp'=4,'kv'=4,'tp'=2] {'kv'}, dimensions={0}, use_global_device_ids=true | all-gather | bytes 655360 | tf_op jit(solution)/shard_map/all_gather | solution.py:142
  41.6 3.8 %fusion.2 = (f32[8,512]{1,0:T(8,128)S(1)}, f32[8,512,640]{2,1,0:T(8,128)S(1)}) fusion(f32[8,640]{1,0:T(8,128)S(1)} %maximum_negate_fusion, pred[512,640]{1,0:T(8,128)(4,1)S(1)} %concatenate.22, bf16[512,8,64]{0,2,1:T(8,128)(2,1)S(1)} %bitcast.94, bf16[640,8,64]{0,2,1:T(8,128)(2,1)} %bitcast.91), kind=kOutput, calls=%fused_computation.6 | convolution fusion | flops 346025984 | bytes 12029952 | tf_op jit(solution)/shard_map/qhd,khd->hqk/dot_general | solution.py:40
  45.4 2.9 %fusion.1 = f32[8,512]{1,0:T(8,128)S(1)} fusion(f32[8,512,640]{2,1,0:T(8,128)S(1)} %get-tuple-element.116, f32[8,512]{1,0:T(8,128)S(1)} %get-tuple-element.115, f32[8,640]{1,0:T(8,128)S(1)} %maximum_negate_fusion, pred[512,640]{1,0:T(8,128)(4,1)S(1)} %concatenate.22), kind=kLoop, calls=%fused_computation.5 | loop fusion | flops 13103104 | bytes 10866688 | tf_op jit(solution)/shard_map/reduce_sum | solution.py:56
  50.0 1.3 %reduce.22 = f32[512,8]{1,0:T(8,128)S(1)} reduce(f32[512,1,8]{2,1,0:T(1,128)S(1)} %bitcast.87, f32[]{:T(128)} %broadcast.115), dimensions={1}, to_apply=%bitcast.60.reduce_sub_computation | reduce | bytes 32772
  52.1 4.0 %all-to-all-start = ((f32[4,1,1024]{2,1,0:T(1,128)}), f32[4,1,1024]{2,1,0:T(1,128)}, u32[]{:S(2)}, u32[]{:S(2)}) async-start(f32[4,1,1024]{2,1,0:T(1,128)} %reshape.272), calls=%async_computation | async-start | bytes 32768 | tf_op jit(solution)/shard_map/all_to_all | solution.py:150
  57.6 2.3 %reduce-window.6 = f32[1,8,8,128]{3,2,1,0:T(8,128)S(1)} reduce-window(f32[1,8,8,128]{3,2,1,0:T(8,128)S(1)} %copy.135, f32[]{:T(128)} %constant.56.clone.1), window={size=1x1x1x128 pad=0_0x0_0x0_0x127_0}, to_apply=%region_10.11 | reduce-window | flops 1040384 | bytes 65540 | tf_op jit(solution)/shard_map/reduce-window
  61.9 1.3 %slice_reduce_fusion.2 = bf16[512]{0:T(512)(128)(2,1)} fusion(bf16[129,512]{1,0:T(8,128)(2,1)} %copy-done.6), kind=kLoop, calls=%fused_computation.58 | loop fusion | bytes 2048 | tf_op jit(solution)/shard_map/slice | solution.py:155
  63.2 2.1 %convolution_convert_fusion.1 = bf16[129,512]{1,0:T(8,128)(2,1)S(1)} fusion(bf16[2048,512]{1,0:T(8,128)(2,1)} %param.24, f32[2048]{0:T(1024)} %param.21, f32[129]{0:T(256)} %copy-done.18, bf16[1,2048]{1,0:T(2,128)(2,1)} %param.20, bf16[128,2048]{1,0:T(8,128)(2,1)S(1)} %copy-done.4), kind=kOutput, calls=%fused_computation.13 | convolution fusion | flops 272448000 | bytes 2766340 | tf_op jit(solution)/shard_map/dot_general | solution.py:121
  66.0 1.1 pad_maximum_fusion.1
  67.1 1.1 copy.129
  68.5 1.5 %copy.134 = bf16[1,1024,512]{1,2,0:T(8,128)(2,1)S(1)} copy(bf16[1,1024,512]{2,1,0:T(8,128)(2,1)} %param.32) | data formatting | bytes 2097152 | tf_op args[13]
  69.9 1.3 %reshape.238 = bf16[8,64]{1,0:T(8,128)(2,1)} reshape(bf16[512]{0:T(512)(128)(2,1)} %slice_reduce_fusion.2) | data formatting | bytes 2048 | tf_op jit(solution)/shard_map/reshape.34
  71.3 6.7 %divide_convert_fusion = bf16[512,8,64]{0,2,1:T(8,128)(2,1)} fusion(bf16[640,8,64]{0,2,1:T(8,128)(2,1)} %bitcast.90, f32[8,512,640]{2,1,0:T(8,128)} %copy-done.1, f32[8,512]{1,0:T(8,128)S(1)} %get-tuple-element.115, f32[8,640]{1,0:T(8,128)S(1)} %copy-done.9, pred[512,640]{1,0:T(8,128)(4,1)S(1)} %concatenate.22, f32[512,8]{0,1:T(8,128)} %bitcast.99), kind=kOutput, calls=%fused_computation.22 | convolution fusion | flops 349175808 | bytes 12046336 | tf_op jit(solution)/shard_map/hqk,khd->qhd/dot_general | solution.py:57
  79.6 1.3 %reduce.24 = f32[512,8]{1,0:T(8,128)S(1)} reduce(f32[512,1,8]{2,1,0:T(1,128)S(1)} %bitcast.88, f32[]{:T(128)} %broadcast.115), dimensions={1}, to_apply=%bitcast.62.reduce_sub_computation | reduce | bytes 32772
  81.7 4.9 %all-to-all-start.1 = ((f32[4,1,1024]{2,1,0:T(1,128)}), f32[4,1,1024]{2,1,0:T(1,128)S(1)}, u32[]{:S(2)}, u32[]{:S(2)}) async-start(f32[4,1,1024]{2,1,0:T(1,128)} %reshape.274), calls=%async_computation.1 | async-start | bytes 32768 | tf_op jit(solution)/shard_map/all_to_all | solution.py:149
  86.5 2.4 %copy.130 = bf16[1,512,512]{2,0,1:T(2,128)(2,1)S(1)} copy(bf16[1,512,512]{1,2,0:T(8,128)(2,1)} %bitcast.92) | data formatting | bytes 1048576 | tf_op jit(solution)/shard_map/broadcast_in_dim;reshape | solution.py:147
  89.5 4.6 %reduce.21 = bf16[512,512]{1,0:T(8,128)(2,1)} reduce(bf16[512,1,512]{2,1,0:T(2,128)(2,1)S(1)} %bitcast.82, bf16[]{:T(256)} %broadcast.114), dimensions={1}, to_apply=%bitcast.58.reduce_sub_computation | reduce | bytes 1048578
  94.1 2.2 %reshape.270 = bf16[4,2,32768]{2,1,0:T(2,128)(2,1)} reshape(bf16[512,512]{1,0:T(8,128)(2,1)} %reduce.21) | data formatting | bytes 1048576
  96.3 1.5 %copy.139 = bf16[1,1024,512]{1,2,0:T(8,128)(2,1)S(1)} copy(bf16[1,1024,512]{2,1,0:T(8,128)(2,1)} %param.33) | data formatting | bytes 2097152 | tf_op args[14]
  97.8 5.1 %all-to-all-start.2 = ((bf16[4,2,32768]{2,1,0:T(2,128)(2,1)}), bf16[4,2,32768]{2,1,0:T(2,128)(2,1)}, u32[]{:S(2)}, u32[]{:S(2)}) async-start(bf16[4,2,32768]{2,1,0:T(2,128)(2,1)} %reshape.270), calls=%async_computation.2 | async-start | bytes 1048576 | tf_op jit(solution)/shard_map/all_to_all | solution.py:147
  104.5 1.4 %reduce.23 = f32[4,1024]{1,0:T(4,128)S(1)} reduce(f32[4,1,1024]{2,1,0:T(1,128)} %all-to-all-done, f32[]{:T(128)} %broadcast.115), dimensions={1}, to_apply=%all_to_all.10.reduce_sub_computation | reduce | bytes 32772 | tf_op jit(solution)/shard_map/all_to_all | solution.py:150
  107.8 5.5 %all-to-all-done.2 = bf16[4,2,32768]{2,1,0:T(2,128)(2,1)} async-done(((bf16[4,2,32768]{2,1,0:T(2,128)(2,1)}), bf16[4,2,32768]{2,1,0:T(2,128)(2,1)}, u32[]{:S(2)}, u32[]{:S(2)}) %all-to-all-start.2) | async-done | bytes 524320 | tf_op jit(solution)/shard_map/all_to_all | solution.py:147
  113.3 2.2 %reshape.271 = bf16[512,1,512]{2,1,0:T(2,128)(2,1)S(1)} reshape(bf16[4,2,32768]{2,1,0:T(2,128)(2,1)} %all-to-all-done.2) | data formatting | bytes 1048576
  115.5 1.1 copy_convert_fusion
  116.6 2.6 %copy.132 = f32[1,512,512]{1,2,0:T(8,128)} copy(f32[1,512,512]{2,1,0:T(8,128)} %copy_convert_fusion) | data formatting | bytes 2097152 | tf_op jit(solution)/shard_map/convert_element_type | solution.py:87
  119.2 1.6 %reshape.241 = f32[4,128,8,64]{1,0,3,2:T(4,128)S(1)} reshape(f32[1,512,512]{1,2,0:T(8,128)} %copy.132) | data formatting | bytes 2097152 | tf_op jit(solution)/shard_map/convert_element_type | solution.py:87
  121.6 2.2 %all_gather.15 = bf16[129,1024]{0,1:T(8,128)(2,1)S(1)} all-gather(bf16[129,512]{0,1:T(8,128)(2,1)S(1)} %pad_maximum_fusion.3), channel_id=1, replica_groups=mesh['dp'=4,'kv'=4,'tp'=2] {'tp'}, dimensions={1}, use_global_device_ids=true | all-gather | bytes 396288 | tf_op jit(solution)/shard_map/all_gather | solution.py:196
  (117 shorter events, 19.7 us)
Async XLA Ops:
  0.6 123.1 %copy-start = (bf16[1024,1024]{1,0:T(8,128)(2,1)S(1)}, bf16[1024,1024]{1,0:T(8,128)(2,1)}, u32[]{:S(2)}) copy-start(bf16[1024,1024]{1,0:T(8,128)(2,1)} %param.27) | copy-start | bytes 6291460
  0.6 3.8 %copy-start.21 = (u32[32]{0:T(128)S(1)}, u32[32]{0:T(128)}, u32[]{:S(2)}) copy-start(u32[32]{0:T(128)} %constant.74) | copy-start | bytes 388
  0.7 19.6 %copy-start.3 = (bf16[128,2048]{1,0:T(8,128)(2,1)S(1)}, bf16[128,2048]{1,0:T(8,128)(2,1)}, u32[]{:S(2)}) copy-start(bf16[128,2048]{1,0:T(8,128)(2,1)} %param.19) | copy-start | bytes 1572868
  0.7 19.6 %copy-start.13 = (bf16[1,2048]{1,0:T(2,128)(2,1)S(1)}, bf16[1,2048]{1,0:T(2,128)(2,1)}, u32[]{:S(2)}) copy-start(bf16[1,2048]{1,0:T(2,128)(2,1)} %param.20) | copy-start | bytes 12292
  0.7 19.6 %copy-start.20 = (f32[2048]{0:T(1024)S(1)}, f32[2048]{0:T(1024)}, u32[]{:S(2)}) copy-start(f32[2048]{0:T(1024)} %param.21) | copy-start | bytes 24580
  0.7 19.3 %copy-start.19 = (f32[16]{0:T(128)S(1)}, f32[16]{0:T(128)}, u32[]{:S(2)}) copy-start(f32[16]{0:T(128)} %param.31) | copy-start | bytes 196
  2.1 21.4 %copy-start.18 = (f32[129]{0:T(256)}, f32[129]{0:T(256)S(1)}, u32[]{:S(2)}) copy-start(f32[129]{0:T(256)S(1)} %add_rsqrt_fusion) | copy-start | bytes 1552
  19.7 2.7 %copy-start.2 = (bf16[512,512]{1,0:T(8,128)(2,1)S(1)}, bf16[512,512]{1,0:T(8,128)(2,1)}, u32[]{:S(2)}) copy-start(bf16[512,512]{1,0:T(8,128)(2,1)} %param.28) | copy-start | bytes 1572868
  22.3 3.5 %copy-start.6 = (bf16[129,512]{1,0:T(8,128)(2,1)}, bf16[129,512]{1,0:T(8,128)(2,1)S(1)}, u32[]{:S(2)}) copy-start(bf16[129,512]{1,0:T(8,128)(2,1)S(1)} %convolution_convert_fusion.2) | copy-start | bytes 396292
  23.5 17.9 %copy-start.12 = (f32[8,512]{1,0:T(8,128)S(1)}, f32[8,512]{1,0:T(8,128)}, u32[]{:S(2)}) copy-start(f32[8,512]{1,0:T(8,128)} %param.30) | copy-start | bytes 49156
  25.8 0.7 copy-start.7
  41.5 3.9 %copy-start.8 = (f32[8,640]{1,0:T(8,128)}, f32[8,640]{1,0:T(8,128)S(1)}, u32[]{:S(2)}) copy-start(f32[8,640]{1,0:T(8,128)S(1)} %maximum_negate_fusion) | copy-start | bytes 61444
  45.3 4.0 %copy-start.1 = (f32[8,512,640]{2,1,0:T(8,128)}, f32[8,512,640]{2,1,0:T(8,128)S(1)}, u32[]{:S(2)}) copy-start(f32[8,512,640]{2,1,0:T(8,128)S(1)} %get-tuple-element.116) | copy-start | bytes 31457284
  45.4 12.2 %copy-start.11 = (f32[1,8,1024]{2,1,0:T(8,128)S(1)}, f32[1,8,1024]{2,1,0:T(8,128)}, u32[]{:S(2)}) copy-start(f32[1,8,1024]{2,1,0:T(8,128)} %param.34) | copy-start | bytes 98308
  45.4 17.8 %copy-start.4 = (bf16[128,2048]{1,0:T(8,128)(2,1)S(1)}, bf16[128,2048]{1,0:T(8,128)(2,1)}, u32[]{:S(2)}) copy-start(bf16[128,2048]{1,0:T(8,128)(2,1)} %param.19) | copy-start | bytes 1572868
  49.3 8.2 %copy-start.10 = (f32[8,512]{1,0:T(8,128)}, f32[8,512]{1,0:T(8,128)S(1)}, u32[]{:S(2)}) copy-start(f32[8,512]{1,0:T(8,128)S(1)} %fusion.1) | copy-start | bytes 49156
  52.1 29.5 %all-to-all-start = ((f32[4,1,1024]{2,1,0:T(1,128)}), f32[4,1,1024]{2,1,0:T(1,128)}, u32[]{:S(2)}, u32[]{:S(2)}) async-start(f32[4,1,1024]{2,1,0:T(1,128)} %reshape.272), calls=%async_computation | async-start | bytes 32768 | tf_op jit(solution)/shard_map/all_to_all | solution.py:150
  57.5 7.8 %copy-start.15 = (pred[1024]{0:T(1024)(128)(4,1)}, pred[1024]{0:T(1024)(128)(4,1)S(1)}, u32[]{:S(2)}) copy-start(pred[1024]{0:T(1024)(128)(4,1)S(1)} %iota_compare_fusion.1) | copy-start | bytes 3076
  65.3 0.7 copy-start.5
  66.0 5.2 %copy-start.9 = (f32[8,640]{1,0:T(8,128)S(1)}, f32[8,640]{1,0:T(8,128)}, u32[]{:S(2)}) copy-start(f32[8,640]{1,0:T(8,128)} %copy-done.8) | copy-start | bytes 61444
  71.2 7.6 %copy-start.14 = (bf16[8,64]{1,0:T(8,128)(2,1)S(1)}, bf16[8,64]{1,0:T(8,128)(2,1)}, u32[]{:S(2)}) copy-start(bf16[8,64]{1,0:T(8,128)(2,1)} %reshape.238) | copy-start | bytes 3076
  71.2 7.8 %copy-start.16 = (pred[1024]{0:T(1024)(128)(4,1)S(1)}, pred[1024]{0:T(1024)(128)(4,1)}, u32[]{:S(2)}) copy-start(pred[1024]{0:T(1024)(128)(4,1)} %copy-done.15) | copy-start | bytes 3076
  71.2 7.8 %copy-start.17 = (f32[8]{0:T(128)S(1)}, f32[8]{0:T(128)}, u32[]{:S(2)}) copy-start(f32[8]{0:T(128)} %slice_reduce_fusion.1) | copy-start | bytes 100
  81.7 16.1 %all-to-all-start.1 = ((f32[4,1,1024]{2,1,0:T(1,128)}), f32[4,1,1024]{2,1,0:T(1,128)S(1)}, u32[]{:S(2)}, u32[]{:S(2)}) async-start(f32[4,1,1024]{2,1,0:T(1,128)} %reshape.274), calls=%async_computation.1 | async-start | bytes 32768 | tf_op jit(solution)/shard_map/all_to_all | solution.py:149
  97.8 15.5 %all-to-all-start.2 = ((bf16[4,2,32768]{2,1,0:T(2,128)(2,1)}), bf16[4,2,32768]{2,1,0:T(2,128)(2,1)}, u32[]{:S(2)}, u32[]{:S(2)}) async-start(bf16[4,2,32768]{2,1,0:T(2,128)(2,1)} %reshape.270), calls=%async_computation.2 | async-start | bytes 1048576 | tf_op jit(solution)/shard_map/all_to_all | solution.py:147
where the time goes:
time: 127 us; the launch traced here: 126 us
  local copies, waits for them, and re-layouts  31.8 us (25%)
  blocking collectives  30.4 us (24%)
  other arithmetic  21.8 us (17%)
  matrix products  19.5 us (15%)
  starting transfers between devices  14 us (11%)
  waiting for transfers between devices  5.55 us (4%)
  between operations  2.56 us (2%)
    all_gather x1, blocking collectives, per_device(): gathered = lax.all_gather(own_queries, 'kv', axis=0, tiled=True)  14.8 us
    unnamed x57, local copies, waits for them, and re-layouts  14.3 us
    unnamed x1, blocking collectives  13.5 us
    unnamed x4, other arithmetic  7.29 us
    dot_general x1, matrix products, one_block(): jnp.einsum('hqk,khd->qhd', exp_scores.astype(jnp.bfloat16), value_heads,...  6.67 us
    all_to_all x1, waiting for transfers between devices, per_device(): lax.all_to_all(part_means[None], 'kv', split_axis=1, concat_axis=0, tiled...  5.54 us
    all_to_all x1, starting transfers between devices, per_device(): lax.all_to_all(part_means[None], 'kv', split_axis=1, concat_axis=0, tiled...  5.1 us
    all_to_all x1, starting transfers between devices, per_device(): lax.all_to_all(part_high[None], 'kv', split_axis=1, concat_axis=0, tiled=...  4.87 us
  transfers between devices with their start and end apart: 3, of which 1 were waited for; matrix products, arithmetic and copies ran while one was open for 32% of the time, Pallas kernels for 0%

commit v1 on v0

v1 whole, which is shorter than its diff:
```python
import functools
import math

import jax
import jax.numpy as jnp
from jax import lax
from jax.experimental import pallas as pl
from jax.experimental.pallas import tpu as pltpu
from jax.sharding import PartitionSpec as P

norm_eps = 1e-06
negative = -1e30
log2e = math.log2(math.e)
MESH = pl.DeviceIdType.MESH
F32 = jnp.float32
BF16 = jnp.bfloat16
NT = (((1,), (1,)), ((), ()))
TN = (((0,), (0,)), ((), ()))


def iota(shape, dim):
    return lax.broadcasted_iota(jnp.int32, shape, dim)


def normalize(rows, gain):
    wide = rows.astype(F32)
    factor = lax.rsqrt(jnp.mean(wide * wide, axis=-1, keepdims=True) + norm_eps)
    return (wide * factor * gain).astype(BF16)


def to_column(row, count):
    eye = iota((count, count), 0) == iota((count, count), 1)
    return jnp.sum(jnp.where(eye, row, 0.0), axis=1, keepdims=True)


def kernel(
    n, heads, width,
    tok, stok, gain, gate_w, gate_b, total_decay, cache_decay, step_gates, step_len,
    wq, wk, wv, wo, cache_k, cache_v, step_k, step_v,
    out_piece, out_step,
    nrm, wq_v, wk_v, wv_v, wo_v, k_all, v_all, sk_v, sv_v,
    q_all, lg, gate_buf, key_bias, mean_buf, stat_buf, att, att_other,
    local_sem, q_send, q_recv, g_send, g_recv, m_send, m_recv, s_send, s_recv, x_send, x_recv,
):
    me = lax.axis_index("kv")
    tp = lax.axis_index("tp")
    rows = tok.shape[0]
    steps = stok.shape[0]
    cache_len = cache_k.shape[0]
    span = step_k.shape[0] // steps
    local = heads * width
    scale = width ** (-0.5) * log2e

    def fetch(index, src, dst):
        copy = pltpu.make_async_copy(src, dst, local_sem.at[index])
        copy.start()
        return copy

    c_wq = fetch(0, wq, wq_v)
    c_wk = fetch(1, wk, wk_v)
    c_wv = fetch(2, wv, wv_v)
    c_ck = fetch(3, cache_k, k_all.at[pl.ds(0, cache_len)])
    c_cv = fetch(4, cache_v, v_all.at[pl.ds(0, cache_len)])
    c_sk = fetch(5, step_k, sk_v)
    c_sv = fetch(6, step_v, sv_v)
    c_wo = fetch(7, wo, wo_v)

    barrier = pltpu.get_barrier_semaphore()

    def greet(d, carry):
        pl.semaphore_signal(
            barrier, inc=1, device_id={"kv": lax.rem(me + d, n)}, device_id_type=MESH
        )
        return carry

    lax.fori_loop(1, n, greet, 0)
    pl.semaphore_signal(barrier, inc=1, device_id={"tp": 1 - tp}, device_id_type=MESH)

    nrm[pl.ds(0, rows)] = normalize(tok[...], gain[...])
    pad = nrm.shape[0] - rows
    step_norm = normalize(stok[...], gain[...]).astype(F32)
    step_rows = jnp.zeros((pad, nrm.shape[1]), F32)
    for b in range(steps):
        step_rows = jnp.where(iota((pad, nrm.shape[1]), 0) == b, step_norm[b : b + 1], step_rows)
    nrm[pl.ds(rows, pad)] = step_rows.astype(BF16)

    c_wq.wait()
    q_new = jnp.dot(nrm[...], wq_v[...], preferred_element_type=F32).astype(BF16)
    q_all[0] = q_new[:rows]
    step_q = q_new[rows:].astype(F32)

    pl.semaphore_wait(barrier, n)

    def q_copy(d):
        return pltpu.make_async_remote_copy(
            src_ref=q_all.at[0], dst_ref=q_all.at[d],
            send_sem=q_send.at[d], recv_sem=q_recv.at[d],
            device_id={"kv": lax.rem(me + d, n)}, device_id_type=MESH,
        )

    def g_copy(d):
        return pltpu.make_async_remote_copy(
            src_ref=gate_buf.at[0], dst_ref=gate_buf.at[d],
            send_sem=g_send.at[d], recv_sem=g_recv.at[d],
            device_id={"kv": lax.rem(me + d, n)}, device_id_type=MESH,
        )

    def m_copy(d):
        return pltpu.make_async_remote_copy(
            src_ref=mean_buf.at[n + d], dst_ref=mean_buf.at[d],
            send_sem=m_send.at[d], recv_sem=m_recv.at[d],
            device_id={"kv": lax.rem(me + n - d, n)}, device_id_type=MESH,
        )

    def s_copy(d):
        return pltpu.make_async_remote_copy(
            src_ref=stat_buf.at[n + d], dst_ref=stat_buf.at[d],
            send_sem=s_send.at[d], recv_sem=s_recv.at[d],
            device_id={"kv": lax.rem(me + n - d, n)}, device_id_type=MESH,
        )

    def each(make):
        def body(d, carry):
            make(d)
            return carry

        lax.fori_loop(1, n, body, 0)

    each(lambda d: q_copy(d).start())

    logits = lax.dot_general(gate_w[...], nrm[...], NT, preferred_element_type=F32)
    logits = logits + to_column(gate_b[...], gate_w.shape[0])
    lg[...] = jnp.minimum(logits, 0.0) - jnp.log1p(jnp.exp(-jnp.abs(logits)))
    own_lg = lg[pl.ds(pl.multiple_of(tp * heads, heads), heads), :]
    piece_lg = own_lg[:, :rows]
    gate_buf[0] = jnp.broadcast_to(jnp.sum(piece_lg, axis=1, keepdims=True), gate_buf.shape[1:])
    each(lambda d: g_copy(d).start())

    c_wk.wait()
    k_new = jnp.dot(nrm[...], wk_v[...], preferred_element_type=F32).astype(BF16)
    k_all[pl.ds(cache_len, rows)] = k_new[:rows]
    step_nk = k_new[rows:].astype(F32)
    c_wv.wait()
    v_new = jnp.dot(nrm[...], wv_v[...], preferred_element_type=F32).astype(BF16)
    v_all[pl.ds(cache_len, rows)] = v_new[:rows]
    step_nv = v_new[rows:].astype(F32)

    upto = (iota((rows, rows), 0) <= iota((rows, rows), 1)).astype(F32)
    running = jnp.dot(
        piece_lg, upto, preferred_element_type=F32, precision=lax.Precision.HIGHEST
    )
    lg_start = to_column(total_decay[...], gate_w.shape[0])
    tp_pick = iota(lg_start.shape, 0)
    start_rows = jnp.where(tp == 0, lg_start[:heads], lg_start[heads : 2 * heads])
    key_bias[:, pl.ds(0, cache_len)] = (start_rows - cache_decay[...]) * log2e

    def add_before(d, total):
        g_copy(d).wait()
        return total + jnp.where(d <= me, gate_buf[d], 0.0)

    before = lax.fori_loop(1, n, add_before, jnp.zeros(gate_buf.shape[1:], F32))
    key_bias[:, pl.ds(cache_len, rows)] = -(before[:, :1] + running) * log2e
    c_ck.wait()
    c_cv.wait()

    pair_lanes = 2 * width
    low_lane = iota((rows, pair_lanes), 1) < width
    stat_lane = iota((rows, 128), 1)
    row_minus_col = iota((rows, rows), 0) - iota((rows, rows), 1)

    def attend(i, carry):
        odd = lax.rem(i, 2)
        d = odd * lax.div(i + 1, 2) + (1 - odd) * lax.rem(n - lax.div(i, 2), n)

        @pl.when(i > 0)
        def _():
            q_copy(d).wait_recv()

        source = lax.rem(me - d + n, n)
        slot = d + n * jnp.minimum(i, 1)
        visible = row_minus_col >= (me - source) * rows
        stats = jnp.zeros((rows, 128), F32)
        for pair in range(heads // 2):
            lanes = pl.ds(pair * pair_lanes, pair_lanes)
            q_pair = q_all[d, :, lanes]
            keys = k_all[:, lanes]
            values = v_all[:, lanes]
            outs = []
            for side in range(2):
                head = 2 * pair + side
                keep = low_lane if side == 0 else jnp.logical_not(low_lane)
                q_one = jnp.where(keep, q_pair, jnp.zeros_like(q_pair))
                scores = lax.dot_general(q_one, keys, NT, preferred_element_type=F32)
                scores = scores * scale + key_bias[head : head + 1, :]
                fresh = jnp.where(visible, scores[:, cache_len:], negative)
                scores = jnp.concatenate([scores[:, :cache_len], fresh], axis=1)
                high = jnp.max(scores, axis=1, keepdims=True)
                weight = jnp.exp2(scores - high)
                mass = jnp.sum(weight, axis=1, keepdims=True)
                mix = jnp.dot(weight.astype(BF16), values, preferred_element_type=F32)
                outs.append(mix / mass)
                stats = jnp.where(stat_lane == head, high, stats)
                stats = jnp.where(stat_lane == heads + head, mass, stats)
            mean_buf[slot, :, lanes] = jnp.where(low_lane, outs[0], outs[1]).astype(BF16)
        stat_buf[slot] = stats.T[: 2 * heads]

        @pl.when(i > 0)
        def _():
            m_copy(d).start()
            s_copy(d).start()

        return carry

    lax.fori_loop(0, n, attend, 0)

    head_mask = lax.div(iota((heads, local), 1), width) == iota((heads, local), 0)
    chunk = 128
    chunks = span // chunk
    later = (iota((chunk, chunk), 0) > iota((chunk, chunk), 1)).astype(F32)
    c_sk.wait()
    c_sv.wait()
    step_att = jnp.zeros((pad, local), F32)
    for b in range(steps):
        length = step_len[b]
        in_cache = iota((heads, span), 1) < length
        kept = jnp.where(in_cache, step_gates[b], 0.0)
        tail = jnp.zeros((heads, 1), F32)
        parts = [None] * chunks
        for c in reversed(range(chunks)):
            piece = kept[:, c * chunk : (c + 1) * chunk]
            inner = jnp.dot(
                piece, later, preferred_element_type=F32, precision=lax.Precision.HIGHEST
            )
            parts[c] = inner + tail
            tail = tail + jnp.sum(piece, axis=1, keepdims=True)
        after = jnp.concatenate(parts, axis=1)
        q_row = jnp.where(head_mask, step_q[b : b + 1], 0.0)
        scores = lax.dot_general(
            q_row.astype(BF16), sk_v[pl.ds(b * span, span)], NT, preferred_element_type=F32
        )
        new_lg = own_lg[:, rows + b : rows + b + 1]
        scores = scores * scale + (new_lg + after) * log2e
        scores = jnp.where(in_cache, scores, negative)
        self_score = jnp.sum(q_row * step_nk[b : b + 1], axis=1, keepdims=True) * scale
        high = jnp.maximum(jnp.max(scores, axis=1, keepdims=True), self_score)
        weight = jnp.exp2(scores - high)
        self_weight = jnp.exp2(self_score - high)
        mass = jnp.sum(weight, axis=1, keepdims=True) + self_weight
        mix = jnp.dot(
            weight.astype(BF16), sv_v[pl.ds(b * span, span)], preferred_element_type=F32
        )
        mix = mix + self_weight.astype(BF16).astype(F32) * step_nv[b : b + 1]
        one = jnp.sum(jnp.where(head_mask, mix / mass, 0.0), axis=0, keepdims=True)
        step_att = jnp.where(iota((pad, local), 0) == b, one, step_att)
    att[pl.ds(rows, pad)] = step_att.astype(BF16)

    def top(d, best):
        s_copy(d).wait()
        return jnp.maximum(best, stat_buf[d, :heads])

    best = lax.fori_loop(1, n, top, stat_buf[0, :heads])

    def share_of(d):
        return stat_buf[d, pl.ds(heads, heads)] * jnp.exp2(stat_buf[d, :heads] - best)

    total = lax.fori_loop(1, n, lambda d, t: t + share_of(d), share_of(0))
    spread = head_mask.astype(F32)

    def weighted(d):
        wide = lax.dot_general(
            share_of(d) / total, spread, TN,
            preferred_element_type=F32, precision=lax.Precision.HIGHEST,
        )
        return wide * mean_buf[d].astype(F32)

    def add_block(d, acc):
        m_copy(d).wait()
        return acc + weighted(d)

    att[pl.ds(0, rows)] = lax.fori_loop(1, n, add_block, weighted(0)).astype(BF16)

    swap = pltpu.make_async_remote_copy(
        src_ref=att, dst_ref=att_other, send_sem=x_send, recv_sem=x_recv,
        device_id={"tp": 1 - tp}, device_id_type=MESH,
    )
    swap.start()
    c_wo.wait()
    mine = pl.ds(pl.multiple_of(tp * local, local), local)
    other = pl.ds(pl.multiple_of((1 - tp) * local, local), local)
    projected = jnp.dot(att[...], wo_v[mine, :], preferred_element_type=F32)
    swap.wait()
    projected = projected + jnp.dot(att_other[...], wo_v[other, :], preferred_element_type=F32)
    out_piece[...] = projected[:rows].astype(BF16)
    out_step[...] = projected[rows : rows + steps].astype(BF16)
    each(lambda d: q_copy(d).wait_send())


def per_device(
    piece_tokens, step_tokens, norm_gain, query_weight, key_weight, value_weight,
    gate_weight, gate_bias, out_weight, cache_keys, cache_values, cache_decay,
    decay_total, step_keys, step_values, step_gates, step_lengths,
):
    n = lax.axis_size("kv")
    rows, model = piece_tokens.shape
    steps = step_tokens.shape[0]
    heads = cache_decay.shape[0]
    local = query_weight.shape[1]
    width = local // heads
    cache_len = cache_keys.shape[0]
    span = step_keys.shape[1]
    columns = out_weight.shape[1]
    padded = rows + 16 * (-(-steps // 16))
    vmem = pl.BlockSpec(memory_space=pltpu.VMEM)
    smem = pl.BlockSpec(memory_space=pltpu.SMEM)
    hbm = pl.BlockSpec(memory_space=pl.ANY)
    dma = pltpu.SemaphoreType.DMA
    piece_out, step_out = pl.pallas_call(
        functools.partial(kernel, n, heads, width),
        out_shape=(
            jax.ShapeDtypeStruct((rows, columns), BF16),
            jax.ShapeDtypeStruct((steps, columns), BF16),
        ),
        in_specs=[vmem] * 8 + [smem] + [hbm] * 8,
        out_specs=(vmem, vmem),
        scratch_shapes=[
            pltpu.VMEM((padded, model), BF16),
            pltpu.VMEM(query_weight.shape, BF16),
            pltpu.VMEM(key_weight.shape, BF16),
            pltpu.VMEM(value_weight.shape, BF16),
            pltpu.VMEM(out_weight.shape, BF16),
            pltpu.VMEM((cache_len + rows, local), BF16),
            pltpu.VMEM((cache_len + rows, local), BF16),
            pltpu.VMEM((steps * span, local), BF16),
            pltpu.VMEM((steps * span, local), BF16),
            pltpu.VMEM((n, rows, local), BF16),
            pltpu.VMEM((gate_weight.shape[1], padded), F32),
            pltpu.VMEM((n, heads, 128), F32),
            pltpu.VMEM((heads, cache_len + rows), F32),
            pltpu.VMEM((2 * n, rows, local), BF16),
            pltpu.VMEM((2 * n, 2 * heads, rows), F32),
            pltpu.VMEM((padded, local), BF16),
            pltpu.VMEM((padded, local), BF16),
            dma((8,)),
            dma((n,)), dma((n,)), dma((n,)), dma((n,)),
            dma((n,)), dma((n,)), dma((n,)), dma((n,)),
            dma(()), dma(()),
        ],
        compiler_params=pltpu.CompilerParams(
            collective_id=0, has_side_effects=True, vmem_limit_bytes=60 * 1024 * 1024
        ),
    )(
        piece_tokens, step_tokens, norm_gain.reshape(1, -1), gate_weight.T,
        gate_bias.reshape(1, -1), decay_total.reshape(1, -1), cache_decay, step_gates,
        step_lengths, query_weight, key_weight, value_weight, out_weight,
        cache_keys, cache_values,
        step_keys.reshape(steps * span, local), step_values.reshape(steps * span, local),
    )
    return piece_out, step_out


def solution(mesh):
    rows = P(("dp", "kv"), None)
    both = P(("dp", "kv"), "tp")
    cols = P(None, "tp")
    in_specs = (
        rows, rows, P(), cols, cols, cols, P(), P(), cols, both, both,
        P("tp", ("dp", "kv")), P("dp"),
        P(("dp", "kv"), None, "tp"), P(("dp", "kv"), None, "tp"),
        P(("dp", "kv"), "tp", None), P(("dp", "kv")),
    )
    return jax.shard_map(
        per_device, mesh=mesh, in_specs=in_specs, out_specs=(both, both), check_vma=False
    )
```

time: 127 us -> 47.4 us (0.37)
  Pallas kernels: 0 us -> 42.9 us
  blocking collectives: 30.4 us -> 0 us
  local copies, waits for them, and re-layouts: 31.8 us -> 2.95 us
  other arithmetic: 21.8 us -> 0 us
  matrix products: 19.5 us -> 0 us
  starting transfers between devices: 14 us -> 0 us
  waiting for transfers between devices: 5.55 us -> 0 us
  between operations: 2.56 us -> 1.29 us
    pallas_call x0 -> x1, Pallas kernels: none -> 42.9 us  [per_device(): pl.pallas_call(functools.partial(kernel, n, heads, width), out_shape=(jax...]
    dot_general x9 -> x0, matrix products: 19.5 us -> none  [the longest x1 6.67 us: one_block(): jnp.einsum('hqk,khd->qhd', exp_scores.astype(jnp.bfloat16), value_heads,...]
    all_gather x2 -> x0, blocking collectives: 16.9 us -> none  [the longest x1 14.8 us: per_device(): gathered = lax.all_gather(own_queries, 'kv', axis=0, tiled=True)]
    all_to_all x3 -> x0, starting transfers between devices: 14 us -> none  [the longest x1 5.1 us: per_device(): lax.all_to_all(part_means[None], 'kv', split_axis=1, concat_axis=0, tiled...]
    unnamed x1 -> x0, blocking collectives: 13.5 us -> none
    unnamed x57 -> x2, local copies, waits for them, and re-layouts: 14.3 us -> 2.95 us
    unnamed x4 -> x0, other arithmetic: 7.29 us -> none
    all_to_all x3 -> x0, waiting for transfers between devices: 5.55 us -> none  [the longest x1 5.54 us: per_device(): lax.all_to_all(part_means[None], 'kv', split_axis=1, concat_axis=0, tiled...]
  transfers between devices with their start and end apart: 3 -> 0, of which waited for: 1 -> 0; matrix products, arithmetic and copies ran while one was open for 32% -> 0% of each run, Pallas kernels for 0% -> 0%
where the time goes in v1:
time: 47.4 us; the launch traced here: 47.1 us
  Pallas kernels  42.9 us (91%)
  local copies, waits for them, and re-layouts  2.95 us (6%)
  between operations  1.29 us (3%)
    pallas_call x1, Pallas kernels, per_device(): pl.pallas_call(functools.partial(kernel, n, heads, width), out_shape=(jax...  42.9 us
    unnamed x2, local copies, waits for them, and re-layouts  2.95 us

profile of v1, /device:TPU:0, one launch (start us, length us, event | category | flops | bytes accessed | tf_op | source)
XLA Modules:
  0.0 47.1 jit_solution(15531703581717441671)
XLA Ops:
  1.3 42.9 %shard_map.176 = (bf16[128,1024]{1,0:T(8,128)(2,1)}, bf16[1,1024]{1,0:T(2,128)(2,1)}) custom-call(bf16[128,2048]{1,0:T(8,128)(2,1)} %tok.1, bf16[1,2048]{1,0:T(2,128)(2,1)} %stok.1, f32[1,2048]{1,0:T(1,128)} %bitcast.9, bf16[16,2048]{1,0:T(8,128)(2,1)} %bitcast.8, f32[1,16]{1,0:T(1,128)} %bitcast.10, f32[1,16]{1,0:T(1,128)} %bitcast.11, ...), custom_call_target="tpu_custom_call" | custom-call | tf_op jit(solution)/shard_map/pallas_call | solution.py:317
  44.2 1.7 %copy.22 = bf16[128,1024]{1,0:T(8,128)(2,1)} copy(bf16[128,1024]{1,0:T(8,128)(2,1)} %get-tuple-element.4) | data formatting | bytes 524288
  45.9 1.3 %copy.23 = bf16[1,1024]{1,0:T(2,128)(2,1)} copy(bf16[1,1024]{1,0:T(2,128)(2,1)} %get-tuple-element.5) | data formatting | bytes 4096

commit v2 on v1

--- a/solution.py
+++ b/solution.py
@@ -18,6 +18,9 @@
 TN = (((0,), (0,)), ((), ()))
 
 
+chunk_count = 2
+
+
 def iota(shape, dim):
     return lax.broadcasted_iota(jnp.int32, shape, dim)
 
@@ -36,11 +39,11 @@
 def kernel(
     n, heads, width,
     tok, stok, gain, gate_w, gate_b, total_decay, cache_decay, step_gates, step_len,
-    wq, wk, wv, wo, cache_k, cache_v, step_k, step_v,
-    out_piece, out_step,
-    nrm, wq_v, wk_v, wv_v, wo_v, k_all, v_all, sk_v, sv_v,
+    wq, wk, wv, cache_k, cache_v, step_k, step_v,
+    out_att,
+    nrm, wq_v, wk_v, wv_v, k_all, k_turned, v_all, sk_v, sv_v,
     q_all, lg, gate_buf, key_bias, mean_buf, stat_buf, att, att_other,
-    local_sem, q_send, q_recv, g_send, g_recv, m_send, m_recv, s_send, s_recv, x_send, x_recv,
+    local_sem, q_right, q_left, q_recv, g_send, g_recv, m_send, m_recv, s_send, s_recv, x_send, x_recv,
 ):
     me = lax.axis_index("kv")
     tp = lax.axis_index("tp")
@@ -59,11 +62,10 @@
     c_wq = fetch(0, wq, wq_v)
     c_wk = fetch(1, wk, wk_v)
     c_wv = fetch(2, wv, wv_v)
-    c_ck = fetch(3, cache_k, k_all.at[pl.ds(0, cache_len)])
+    c_ck = fetch(3, cache_k, k_all)
     c_cv = fetch(4, cache_v, v_all.at[pl.ds(0, cache_len)])
     c_sk = fetch(5, step_k, sk_v)
     c_sv = fetch(6, step_v, sv_v)
-    c_wo = fetch(7, wo, wo_v)
 
     barrier = pltpu.get_barrier_semaphore()
 
@@ -86,17 +88,28 @@
 
     c_wq.wait()
     q_new = jnp.dot(nrm[...], wq_v[...], preferred_element_type=F32).astype(BF16)
-    q_all[0] = q_new[:rows]
+    part = local // chunk_count
+    for c in range(chunk_count):
+        q_all[me, c] = q_new[:rows, c * part : (c + 1) * part]
     step_q = q_new[rows:].astype(F32)
 
     pl.semaphore_wait(barrier, n)
 
-    def q_copy(d):
+    def q_copy(source, c, step, sems):
         return pltpu.make_async_remote_copy(
-            src_ref=q_all.at[0], dst_ref=q_all.at[d],
-            send_sem=q_send.at[d], recv_sem=q_recv.at[d],
-            device_id={"kv": lax.rem(me + d, n)}, device_id_type=MESH,
-        )
+            src_ref=q_all.at[source, c], dst_ref=q_all.at[source, c],
+            send_sem=sems.at[source, c], recv_sem=q_recv.at[source, c],
+            device_id={"kv": lax.rem(me + step + n, n)}, device_id_type=MESH,
+        )
+
+    def to_right(source, c):
+        return q_copy(source, c, 1, q_right)
+
+    def to_left(source, c):
+        return q_copy(source, c, -1, q_left)
+
+    has_right = me < n - 1
+    has_left = me > 0
 
     def g_copy(d):
         return pltpu.make_async_remote_copy(
@@ -126,7 +139,14 @@
 
         lax.fori_loop(1, n, body, 0)
 
-    each(lambda d: q_copy(d).start())
+    for c in range(chunk_count):
+        @pl.when(has_right)
+        def _():
+            to_right(me, c).start()
+
+        @pl.when(has_left)
+        def _():
+            to_left(me, c).start()
 
     logits = lax.dot_general(gate_w[...], nrm[...], NT, preferred_element_type=F32)
     logits = logits + to_column(gate_b[...], gate_w.shape[0])
@@ -136,9 +156,11 @@
     gate_buf[0] = jnp.broadcast_to(jnp.sum(piece_lg, axis=1, keepdims=True), gate_buf.shape[1:])
     each(lambda d: g_copy(d).start())
 
+    c_ck.wait()
+    k_turned[:, pl.ds(0, cache_len)] = k_all[...].T
     c_wk.wait()
     k_new = jnp.dot(nrm[...], wk_v[...], preferred_element_type=F32).astype(BF16)
-    k_all[pl.ds(cache_len, rows)] = k_new[:rows]
+    k_turned[:, pl.ds(cache_len, rows)] = k_new[:rows].T
     step_nk = k_new[rows:].astype(F32)
     c_wv.wait()
     v_new = jnp.dot(nrm[...], wv_v[...], preferred_element_type=F32).astype(BF16)
@@ -150,7 +172,6 @@
         piece_lg, upto, preferred_element_type=F32, precision=lax.Precision.HIGHEST
     )
     lg_start = to_column(total_decay[...], gate_w.shape[0])
-    tp_pick = iota(lg_start.shape, 0)
     start_rows = jnp.where(tp == 0, lg_start[:heads], lg_start[heads : 2 * heads])
     key_bias[:, pl.ds(0, cache_len)] = (start_rows - cache_decay[...]) * log2e
 
@@ -160,37 +181,31 @@
 
     before = lax.fori_loop(1, n, add_before, jnp.zeros(gate_buf.shape[1:], F32))
     key_bias[:, pl.ds(cache_len, rows)] = -(before[:, :1] + running) * log2e
-    c_ck.wait()
-    c_cv.wait()
 
     pair_lanes = 2 * width
     low_lane = iota((rows, pair_lanes), 1) < width
     stat_lane = iota((rows, 128), 1)
     row_minus_col = iota((rows, rows), 0) - iota((rows, rows), 1)
 
-    def attend(i, carry):
-        odd = lax.rem(i, 2)
-        d = odd * lax.div(i + 1, 2) + (1 - odd) * lax.rem(n - lax.div(i, 2), n)
-
-        @pl.when(i > 0)
-        def _():
-            q_copy(d).wait_recv()
-
-        source = lax.rem(me - d + n, n)
-        slot = d + n * jnp.minimum(i, 1)
+    c_cv.wait()
+
+    def attend(d, source, remote):
+        slot = d + n if remote else d
         visible = row_minus_col >= (me - source) * rows
         stats = jnp.zeros((rows, 128), F32)
+        pairs_in_part = heads // 2 // chunk_count
         for pair in range(heads // 2):
             lanes = pl.ds(pair * pair_lanes, pair_lanes)
-            q_pair = q_all[d, :, lanes]
-            keys = k_all[:, lanes]
+            inner = pl.ds(pair % pairs_in_part * pair_lanes, pair_lanes)
+            q_pair = q_all[source, pair // pairs_in_part, :, inner]
+            keys = k_turned[lanes, :]
             values = v_all[:, lanes]
             outs = []
             for side in range(2):
                 head = 2 * pair + side
                 keep = low_lane if side == 0 else jnp.logical_not(low_lane)
                 q_one = jnp.where(keep, q_pair, jnp.zeros_like(q_pair))
-                scores = lax.dot_general(q_one, keys, NT, preferred_element_type=F32)
+                scores = jnp.dot(q_one, keys, preferred_element_type=F32)
                 scores = scores * scale + key_bias[head : head + 1, :]
                 fresh = jnp.where(visible, scores[:, cache_len:], negative)
                 scores = jnp.concatenate([scores[:, :cache_len], fresh], axis=1)
@@ -203,15 +218,43 @@
                 stats = jnp.where(stat_lane == heads + head, mass, stats)
             mean_buf[slot, :, lanes] = jnp.where(low_lane, outs[0], outs[1]).astype(BF16)
         stat_buf[slot] = stats.T[: 2 * heads]
-
-        @pl.when(i > 0)
-        def _():
+        if remote:
             m_copy(d).start()
             s_copy(d).start()
 
+    def step(k, carry):
+        for c in range(chunk_count):
+            @pl.when(me >= k)
+            def _():
+                to_right(me - k, c).wait_recv()
+
+                @pl.when(has_right)
+                def _():
+                    to_right(me - k, c).start()
+
+            @pl.when(me + k < n)
+            def _():
+                to_left(me + k, c).wait_recv()
+
+                @pl.when(has_left)
+                def _():
+                    to_left(me + k, c).start()
+
+        @pl.when(me >= k)
+        def _():
+            attend(k, me - k, True)
+
+        @pl.when(me + k < n)
+        def _():
+            attend(n - k, me + k, True)
+
+        @pl.when(k == 1)
+        def _():
+            attend(0, me, False)
+
         return carry
 
-    lax.fori_loop(0, n, attend, 0)
+    lax.fori_loop(1, n, step, 0)
 
     head_mask = lax.div(iota((heads, local), 1), width) == iota((heads, local), 0)
     chunk = 128
@@ -284,15 +327,31 @@
         device_id={"tp": 1 - tp}, device_id_type=MESH,
     )
     swap.start()
-    c_wo.wait()
     mine = pl.ds(pl.multiple_of(tp * local, local), local)
     other = pl.ds(pl.multiple_of((1 - tp) * local, local), local)
-    projected = jnp.dot(att[...], wo_v[mine, :], preferred_element_type=F32)
+    out_att[:, mine] = att[...]
     swap.wait()
-    projected = projected + jnp.dot(att_other[...], wo_v[other, :], preferred_element_type=F32)
+    out_att[:, other] = att_other[...]
+
+    def sent(source, carry):
+        for c in range(chunk_count):
+            @pl.when(jnp.logical_and(has_right, source <= me))
+            def _():
+                to_right(source, c).wait_send()
+
+            @pl.when(jnp.logical_and(has_left, source >= me))
+            def _():
+                to_left(source, c).wait_send()
+
+        return carry
+
+    lax.fori_loop(0, n, sent, 0)
+
+
+def project(rows, att, weight, out_piece, out_step):
+    projected = jnp.dot(att[...], weight[...], preferred_element_type=F32)
     out_piece[...] = projected[:rows].astype(BF16)
-    out_step[...] = projected[rows : rows + steps].astype(BF16)
-    each(lambda d: q_copy(d).wait_send())
+    out_step[...] = projected[rows : rows + out_step.shape[0]].astype(BF16)
 
 
 def per_device(
@@ -312,27 +371,24 @@
     padded = rows + 16 * (-(-steps // 16))
     vmem = pl.BlockSpec(memory_space=pltpu.VMEM)
     smem = pl.BlockSpec(memory_space=pltpu.SMEM)
-    hbm = pl.BlockSpec(memory_space=pl.ANY)
+    hbm = pl.BlockSpec(memory_space=pltpu.HBM)
     dma = pltpu.SemaphoreType.DMA
-    piece_out, step_out = pl.pallas_call(
+    att = pl.pallas_call(
         functools.partial(kernel, n, heads, width),
-        out_shape=(
-            jax.ShapeDtypeStruct((rows, columns), BF16),
-            jax.ShapeDtypeStruct((steps, columns), BF16),
-        ),
-        in_specs=[vmem] * 8 + [smem] + [hbm] * 8,
-        out_specs=(vmem, vmem),
+        out_shape=jax.ShapeDtypeStruct((padded, out_weight.shape[0]), BF16),
+        in_specs=[vmem] * 8 + [smem] + [hbm] * 7,
+        out_specs=vmem,
         scratch_shapes=[
             pltpu.VMEM((padded, model), BF16),
             pltpu.VMEM(query_weight.shape, BF16),
             pltpu.VMEM(key_weight.shape, BF16),
             pltpu.VMEM(value_weight.shape, BF16),
-            pltpu.VMEM(out_weight.shape, BF16),
-            pltpu.VMEM((cache_len + rows, local), BF16),
+            pltpu.VMEM((cache_len, local), BF16),
+            pltpu.VMEM((local, cache_len + rows), BF16),
             pltpu.VMEM((cache_len + rows, local), BF16),
             pltpu.VMEM((steps * span, local), BF16),
             pltpu.VMEM((steps * span, local), BF16),
-            pltpu.VMEM((n, rows, local), BF16),
+            pltpu.VMEM((n, chunk_count, rows, local // chunk_count), BF16),
             pltpu.VMEM((gate_weight.shape[1], padded), F32),
             pltpu.VMEM((n, heads, 128), F32),
             pltpu.VMEM((heads, cache_len + rows), F32),
@@ -340,8 +396,9 @@
             pltpu.VMEM((2 * n, 2 * heads, rows), F32),
             pltpu.VMEM((padded, local), BF16),
             pltpu.VMEM((padded, local), BF16),
-            dma((8,)),
-            dma((n,)), dma((n,)), dma((n,)), dma((n,)),
+            dma((7,)),
+            dma((n, chunk_count)), dma((n, chunk_count)), dma((n, chunk_count)),
+            dma((n,)), dma((n,)),
             dma((n,)), dma((n,)), dma((n,)), dma((n,)),
             dma(()), dma(()),
         ],
@@ -351,11 +408,20 @@
     )(
         piece_tokens, step_tokens, norm_gain.reshape(1, -1), gate_weight.T,
         gate_bias.reshape(1, -1), decay_total.reshape(1, -1), cache_decay, step_gates,
-        step_lengths, query_weight, key_weight, value_weight, out_weight,
+        step_lengths, query_weight, key_weight, value_weight,
         cache_keys, cache_values,
         step_keys.reshape(steps * span, local), step_values.reshape(steps * span, local),
     )
-    return piece_out, step_out
+    return pl.pallas_call(
+        functools.partial(project, rows),
+        out_shape=(
+            jax.ShapeDtypeStruct((rows, columns), BF16),
+            jax.ShapeDtypeStruct((steps, columns), BF16),
+        ),
+        in_specs=[vmem, vmem],
+        out_specs=(vmem, vmem),
+        compiler_params=pltpu.CompilerParams(vmem_limit_bytes=16 * 1024 * 1024),
+    )(att, out_weight)
 
 
 def solution(mesh):

time: 47.4 us -> 39.1 us (0.82)
  Pallas kernels: 42.9 us -> 36.6 us
  local copies, waits for them, and re-layouts: 2.95 us -> 0.96 us
    pallas_call x1 -> x2, Pallas kernels: 42.9 us -> 36.6 us  [the longest x1 35.4 us: per_device(): pl.pallas_call(functools.partial(kernel, n, heads, width), out_shape=jax....]
    unnamed x2 -> x4, local copies, waits for them, and re-layouts: 2.95 us -> 0.96 us
where the time goes in v2:
time: 39.1 us; the launch traced here: 38.9 us
  Pallas kernels  36.6 us (94%)
  between operations  1.32 us (3%)
  local copies, waits for them, and re-layouts  0.96 us (2%)
    pallas_call x1, Pallas kernels, per_device(): pl.pallas_call(functools.partial(kernel, n, heads, width), out_shape=jax....  35.4 us
    pallas_call x1, Pallas kernels, per_device(): pl.pallas_call(functools.partial(project, rows), out_shape=(jax.ShapeDtyp...  1.19 us
    unnamed x4, local copies, waits for them, and re-layouts  0.96 us

profile of v2, /device:TPU:0, one launch (start us, length us, event | category | flops | bytes accessed | tf_op | source)
XLA Modules:
  0.0 38.9 jit_solution(4513510373686740028)
XLA Ops:
  1.3 0.0 copy-start
  1.3 35.4 %shard_map.176.att = bf16[144,1024]{1,0:T(8,128)(2,1)} custom-call(bf16[128,2048]{1,0:T(8,128)(2,1)} %tok.1, bf16[1,2048]{1,0:T(2,128)(2,1)} %stok.1, f32[1,2048]{1,0:T(1,128)} %bitcast.9, bf16[16,2048]{1,0:T(8,128)(2,1)} %bitcast.8, f32[1,16]{1,0:T(1,128)} %bitcast.10, f32[1,16]{1,0:T(1,128)} %bitcast.11, f32[8,512]{1,0:T(8,128)} %cache_decay.1, ...), custom_call_target="tpu_custom_call" | custom-call | tf_op jit(solution)/shard_map/pallas_call | solution.py:376
  36.7 0.0 copy-done
  36.7 0.0 copy-start.1
  36.7 1.0 %copy-done.1 = bf16[144,1024]{1,0:T(8,128)(2,1)S(1)} copy-done((bf16[144,1024]{1,0:T(8,128)(2,1)S(1)}, bf16[144,1024]{1,0:T(8,128)(2,1)}, u32[]{:S(2)}) %copy-start.1) | copy-done | bytes 294936
  37.7 1.2 %shard_map.177 = (bf16[128,1024]{1,0:T(8,128)(2,1)}, bf16[1,1024]{1,0:T(2,128)(2,1)}) custom-call(bf16[144,1024]{1,0:T(8,128)(2,1)S(1)} %copy-done.1, bf16[1024,1024]{1,0:T(8,128)(2,1)S(1)} %copy-done), custom_call_target="tpu_custom_call" | custom-call | tf_op jit(solution)/shard_map/pallas_call | solution.py:415
Async XLA Ops:
  1.3 35.4 %copy-start = (bf16[1024,1024]{1,0:T(8,128)(2,1)S(1)}, bf16[1024,1024]{1,0:T(8,128)(2,1)}, u32[]{:S(2)}) copy-start(bf16[1024,1024]{1,0:T(8,128)(2,1)} %weight.1) | copy-start | bytes 6291460
  36.7 1.0 %copy-start.1 = (bf16[144,1024]{1,0:T(8,128)(2,1)S(1)}, bf16[144,1024]{1,0:T(8,128)(2,1)}, u32[]{:S(2)}) copy-start(bf16[144,1024]{1,0:T(8,128)(2,1)} %shard_map.176.att) | copy-start | bytes 884740
